TPU v7x, 32 devices: a whole 2x2x4 slice. The times are simulated.
32 devices in a mesh: sp: 16 (over z, y, x), tp: 2 (over core).
Axes of the slice: x: 2, y: 2, z: 4, core: 2. Of those that a mesh axis runs over, the one named last changes fastest.
Arguments:
- queries: bfloat16 [3072, 1024], P('sp', 'tp'), may hold values from -6 to 6
- keys: bfloat16 [3072, 512], P('sp', 'tp'), may hold values from -6 to 6
- values: bfloat16 [3072, 512], P('sp', 'tp'), may hold values from -6 to 6
- query_gain: float32 [16, 64], P('tp'), may hold values from 1.4 to 7.5
- key_gain: float32 [8, 64], P('tp'), may hold values from 1.4 to 7.5
- out_weight: bfloat16 [1024, 2048], P('tp'), may hold values from -0.375 to 0.375
- residual: bfloat16 [3072, 2048], P('sp'), may hold values from -170 to 170
- norm_gain: float32 [2048], replicated, may hold values from 0.1 to 1.9
- gate_weight: bfloat16 [2048, 5632], P('sp', 'tp'), may hold values from -0.125 to 0.125
- up_weight: bfloat16 [2048, 5632], P('sp', 'tp'), may hold values from -0.125 to 0.125
- down_weight: bfloat16 [5632, 2048], P('tp', 'sp'), may hold values from -0.15625 to 0.15625
Outputs:
- mixed: bfloat16 [3072, 2048], P('sp')
All inputs are finite; a program needn't handle non-finite values.
Results may differ from a plain program's by a relative error of at most 0.017.
Values may be sent and summed in bfloat16 or wider, within the bound.
A program may use at most 128 MiB of HBM per device.

v0:
```python
import jax
import jax.numpy as jnp
from jax import lax
from jax.sharding import PartitionSpec as P

GRID_W = 64
epsilon = 1e-06
rope_base = 10000.0
block_keys = 2048


def rotate_pairs(entries, places):
    half = entries.shape[-1] // 2
    frequency = rope_base ** (-jnp.arange(half, dtype=jnp.float32) / half)
    angle = places.astype(jnp.float32)[:, None, None] * frequency[None, None, :]
    cosine = jnp.cos(angle)
    sine = jnp.sin(angle)
    first = entries[..., :half]
    second = entries[..., half:]
    return jnp.concatenate(
        [first * cosine - second * sine, first * sine + second * cosine], axis=-1
    )


def grid_rotate(entries, grid_rows, grid_cols):
    half = entries.shape[-1] // 2
    return jnp.concatenate(
        [
            rotate_pairs(entries[..., :half], grid_rows),
            rotate_pairs(entries[..., half:], grid_cols),
        ],
        axis=-1,
    )


def head_norm(entries, gains):
    factor = lax.rsqrt(jnp.mean(entries * entries, axis=-1, keepdims=True) + epsilon)
    return entries * factor * gains[None]


def row_norm(mid, norm_gain):
    wide = mid.astype(jnp.float32)
    return (
        wide * lax.rsqrt(jnp.mean(wide * wide, axis=-1, keepdims=True) + epsilon) * norm_gain
    ).astype(jnp.bfloat16)


def block_span(length):
    if length <= block_keys:
        return length
    span = block_keys
    while length % span != 0:
        span = span - 1
    return span


def body(
    queries,
    keys,
    values,
    query_gain,
    key_gain,
    out_weight,
    residual,
    norm_gain,
    gate_weight,
    up_weight,
    down_weight,
):
    own = queries.shape[0]
    heads = query_gain.shape[0]
    key_heads = key_gain.shape[0]
    head_size = query_gain.shape[1]
    group = heads // key_heads
    gate_full, up_full, down_full = (
        lax.all_gather(gate_weight, "sp", axis=0, tiled=True),
        lax.all_gather(up_weight, "sp", axis=0, tiled=True),
        lax.all_gather(down_weight, "sp", axis=1, tiled=True),
    )
    places = lax.axis_index("sp") * own + jnp.arange(own, dtype=jnp.int32)
    grid_rows = places // GRID_W
    grid_cols = places % GRID_W
    query_turned = grid_rotate(
        head_norm(queries.astype(jnp.float32).reshape(own, heads, head_size), query_gain),
        grid_rows,
        grid_cols,
    ).astype(jnp.bfloat16)
    query_groups = query_turned.reshape(own, key_heads, group, head_size)
    key_turned = (
        grid_rotate(
            head_norm(keys.astype(jnp.float32).reshape(own, key_heads, head_size), key_gain),
            grid_rows,
            grid_cols,
        )
        .astype(jnp.bfloat16)
        .reshape(own, key_heads * head_size)
    )
    scale = head_size ** (-0.5)

    def absorb(carry, key_block, value_block):
        top, total, summed = carry
        key_block = key_block.reshape(-1, key_heads, head_size)
        value_block = value_block.reshape(-1, key_heads, head_size)
        score = (
            jnp.einsum(
                "qgrd,kgd->qgrk", query_groups, key_block, preferred_element_type=jnp.float32
            )
            * scale
        )
        new_top = jnp.maximum(top, jnp.max(score, axis=-1))
        weight = jnp.exp(score - new_top[..., None])
        shrink = jnp.exp(top - new_top)
        total = total * shrink + jnp.sum(weight, axis=-1)
        summed = summed * shrink[..., None] + jnp.einsum(
            "qgrk,kgd->qgrd",
            weight.astype(jnp.bfloat16),
            value_block,
            preferred_element_type=jnp.float32,
        )
        return (new_top, total, summed)

    def fold_keys(carry, pieces):
        length = pieces[0].shape[0]
        span = block_span(length)
        if span == length:
            return absorb(carry, pieces[0], pieces[1])
        width = pieces[0].shape[1]
        key_blocks = pieces[0].reshape(length // span, span, width)
        value_blocks = pieces[1].reshape(length // span, span, width)

        def scan_step(inner, blocks):
            return (absorb(inner, blocks[0], blocks[1]), None)

        result, unused = lax.scan(scan_step, carry, (key_blocks, value_blocks))
        return result

    start_state = (
        jnp.full((own, key_heads, group), -jnp.inf, jnp.float32),
        jnp.zeros((own, key_heads, group), jnp.float32),
        jnp.zeros((own, key_heads, group, head_size), jnp.float32),
    )
    top, total, summed = fold_keys(
        start_state,
        (
            lax.all_gather(key_turned, "sp", axis=0, tiled=True),
            lax.all_gather(values, "sp", axis=0, tiled=True),
        ),
    )
    attended = (summed / total[..., None]).reshape(own, heads * head_size).astype(jnp.bfloat16)
    part_rows = own // lax.axis_size("tp")
    branch = lax.psum_scatter(
        jnp.dot(
            lax.slice_in_dim(attended, 0, lax.axis_size("tp") * part_rows, axis=0),
            out_weight,
            preferred_element_type=jnp.float32,
        ).astype(jnp.bfloat16),
        "tp",
        scatter_dimension=0,
        tiled=True,
    ).astype(jnp.float32)
    own_rows = lax.dynamic_slice_in_dim(residual, lax.axis_index("tp") * part_rows, part_rows, 0)
    mid = (own_rows.astype(jnp.float32) + branch).astype(jnp.bfloat16)
    normed_all = lax.all_gather(row_norm(mid, norm_gain), "tp", axis=0, tiled=True)
    gate = jnp.dot(normed_all, gate_full, preferred_element_type=jnp.float32)
    up_value = jnp.dot(normed_all, up_full, preferred_element_type=jnp.float32)
    hidden = (jax.nn.silu(gate) * up_value).astype(jnp.bfloat16)
    terms = jnp.dot(hidden, down_full, preferred_element_type=jnp.float32)
    ffn = lax.psum_scatter(
        terms.astype(jnp.bfloat16), "tp", scatter_dimension=0, tiled=True
    ).astype(jnp.float32)
    finished = (mid.astype(jnp.float32) + ffn).astype(jnp.bfloat16)
    return lax.all_gather(finished, "tp", axis=0, tiled=True)


def solution(mesh):
    in_specs = (
        P("sp", "tp"),
        P("sp", "tp"),
        P("sp", "tp"),
        P("tp", None),
        P("tp", None),
        P("tp", None),
        P("sp", None),
        P(),
        P("sp", "tp"),
        P("sp", "tp"),
        P("tp", "sp"),
    )
    out_specs = P("sp", None)
    return jax.shard_map(body, mesh=mesh, in_specs=in_specs, out_specs=out_specs, check_vma=False)
```

profile of v0, /device:TPU:0, one launch (start us, length us, event | category | flops | bytes accessed | tf_op | source)
XLA Modules:
  0.0 684.2 jit_solution(15495165526293549305)
XLA Ops:
  6.6 1.1 copy.22
  7.8 0.8 fusion.22
  8.6 0.2 multiply_cosine_fusion.1
  8.8 0.7 copy.23
  9.6 0.0 all-gather.8.cloned.1.call-start
  9.7 0.7 all-gather.8.cloned.1.call-update
  10.4 0.0 reduce-scatter.3.cloned.1.call-start
  10.4 1.1 copy.24
  11.5 0.1 fusion.19
  11.6 0.8 fusion.20
  12.4 0.1 subtract_convert_fusion.1
  12.5 0.7 pad_maximum_fusion
  13.3 57.5 %all-gather.6.cloned.1.call-done = bf16[3072,256]{1,0:T(8,128)(2,1)} async-done(((bf16[192,256]{1,0:T(8,128)(2,1)}), bf16[3072,256]{1,0:T(8,128)(2,1)}) %all-gather.6.cloned.1.call-update) | async-done | bytes 1572880 | tf_op jit(solution)/shard_map/all_gather | solution.py:145
  70.8 59.5 %all-gather.8.cloned.1.call-done = bf16[3072,256]{1,0:T(8,128)(2,1)} async-done(((bf16[192,256]{1,0:T(8,128)(2,1)}), bf16[3072,256]{1,0:T(8,128)(2,1)}) %all-gather.8.cloned.1.call-update) | async-done | bytes 1572880 | tf_op jit(solution)/shard_map/all_gather | solution.py:146
  130.3 43.6 %while.15 = (s32[]{:T(128)}, f32[192,4,2]{0,2,1:T(2,128)S(1)}, f32[192,4,2]{0,2,1:T(2,128)S(1)}, f32[192,4,2,64]{0,3,2,1:T(8,128)S(1)}, bf16[2,1536,256]{2,1,0:T...) while((s32[]{:T(128)}, f32[192,4,2]{0,2,1:T(2,128)S(1)}, ...), condition=%wide.region_5.6_spmd.clone, body=%wide.region_2.5_spmd.clone.sunk | while | flops 623156736 | bytes 37257324 | solution.py:134
  130.3 2.6 constant_dynamic-slice_fusion.3
  132.9 1.4 copy.33
  134.3 6.0 bitcast_reduce_fusion.2
  140.4 5.4 fusion.51
  145.8 1.4 copy.34
  147.2 4.8 fusion.53
  152.1 2.6 constant_dynamic-slice_fusion.3
  154.7 1.4 copy.33
  156.1 6.0 bitcast_reduce_fusion.2
  162.1 5.4 fusion.51
  167.6 1.4 copy.34
  169.0 4.8 fusion.53
  173.9 0.1 divide_convert_fusion
  173.9 1.5 convolution_convert_fusion.1
  175.4 0.0 all-gather.10.cloned.1.call-start
  175.5 0.5 all-gather.10.cloned.1.call-update
  176.0 0.0 all-gather.12.cloned.1.call-start
  176.1 0.5 all-gather.12.cloned.1.call-update
  176.7 0.5 all-gather.14.cloned.1.call-update
  177.2 0.0 reduce-scatter.5.cloned.1.call-start
  177.2 5.2 reduce-scatter.3.cloned.1.call-done
  182.5 1.4 fusion.15
  183.9 0.2 fusion.17
  184.0 2.5 all_gather.23
  186.6 141.1 %all-gather.10.cloned.1.call-done = bf16[2048,2816]{1,0:T(8,128)(2,1)} async-done(((bf16[128,2816]{1,0:T(8,128)(2,1)}), bf16[2048,2816]{1,0:T(8,128)(2,1)}) %all-gather.10.cloned.1.call-update) | async-done | bytes 11534352 | tf_op jit(solution)/shard_map/all_gather | solution.py:76
  327.6 8.0 %fusion.27 = f32[192,2816]{1,0:T(8,128)} fusion(bf16[192,2048]{1,0:T(8,128)(2,1)S(1)} %all_gather.23, bf16[2048,2816]{1,0:T(8,128)(2,1)} %all-gather.10.cloned.1.call-done), kind=kOutput, calls=%fused_computation.67 | convolution fusion | flops 2214592512 | bytes 14483456 | tf_op jit(solution)/shard_map/dot_general | solution.py:164
  335.7 134.2 %all-gather.12.cloned.1.call-done = bf16[2048,2816]{1,0:T(8,128)(2,1)} async-done(((bf16[128,2816]{1,0:T(8,128)(2,1)}), bf16[2048,2816]{1,0:T(8,128)(2,1)}) %all-gather.12.cloned.1.call-update) | async-done | bytes 11534352 | tf_op jit(solution)/shard_map/all_gather | solution.py:77
  469.9 182.8 %all-gather.14.cloned.1.call-done = bf16[2816,2048]{1,0:T(8,128)(2,1)} async-done(((bf16[2816,128]{1,0:T(8,128)(2,1)}), bf16[2816,2048]{1,0:T(8,128)(2,1)}) %all-gather.14.cloned.1.call-update) | async-done | bytes 11534352 | tf_op jit(solution)/shard_map/all_gather | solution.py:78
  652.7 13.8 %convolution_convert_fusion = bf16[192,2048]{1,0:T(8,128)(2,1)} fusion(bf16[2816,2048]{1,0:T(8,128)(2,1)} %all-gather.14.cloned.1.call-done, bf16[192,2048]{1,0:T(8,128)(2,1)S(1)} %all_gather.23, bf16[2048,2816]{1,0:T(8,128)(2,1)} %all-gather.12.cloned.1.call-done, f32[192,2816]{1,0:T(8,128)} %fusion.27), kind=kOutput, calls=%fused_computation.19 | convolution fusion | flops 4432822272 | bytes 26804224 | tf_op jit(solution)/shard_map/dot_general | solution.py:167
  666.5 6.5 reduce-scatter.5.cloned.1.call-done
  673.0 1.1 fusion.18
  674.1 2.4 all_gather.27
  676.5 0.9 copy.48
  (26 shorter events, 0.3 us)
Async XLA Ops:
  6.5 167.4 %copy-start = (bf16[512,2048]{1,0:T(8,128)(2,1)S(1)}, bf16[512,2048]{1,0:T(8,128)(2,1)}, u32[]{:S(2)}) copy-start(bf16[512,2048]{1,0:T(8,128)(2,1)} %param.18) | copy-start | bytes 6291460
  6.5 64.3 %all-gather.6.cloned.1.call-start = ((), (), s32[]{:S(2)}) async-start(), calls=%async_computation.2 | async-start | bytes 1671168 | tf_op jit(solution)/shard_map/all_gather | solution.py:145
  9.6 120.7 %all-gather.8.cloned.1.call-start = ((), (), s32[]{:S(2)}) async-start(), calls=%async_computation.3 | async-start | bytes 1671168 | tf_op jit(solution)/shard_map/all_gather | solution.py:146
  10.4 172.1 %reduce-scatter.3.cloned.1.call-start = ((), (), s32[]{:S(2)}) async-start(), calls=%async_computation.4 | async-start | bytes 1179648 | tf_op jit(solution)/shard_map/reduce_scatter | solution.py:151
  130.3 53.6 %copy-start.1 = (f32[2048]{0:T(1024)S(1)}, f32[2048]{0:T(1024)}, u32[]{:S(2)}) copy-start(f32[2048]{0:T(1024)} %param.20) | copy-start | bytes 24580
  175.4 152.2 %all-gather.10.cloned.1.call-start = ((), (), s32[]{:S(2)}) async-start(), calls=%async_computation.5 | async-start | bytes 12255232 | tf_op jit(solution)/shard_map/all_gather | solution.py:76
  176.0 293.9 %all-gather.12.cloned.1.call-start = ((), (), s32[]{:S(2)}) async-start(), calls=%async_computation.6 | async-start | bytes 12255232 | tf_op jit(solution)/shard_map/all_gather | solution.py:77
  176.6 476.1 %all-gather.14.cloned.1.call-start = ((), (), s32[]{:S(2)}) async-start(), calls=%async_computation.7 | async-start | bytes 12255232 | tf_op jit(solution)/shard_map/all_gather | solution.py:78
  177.2 495.9 %reduce-scatter.5.cloned.1.call-start = ((), (), s32[]{:S(2)}) async-start(), calls=%async_computation.8 | async-start | bytes 1179648 | tf_op jit(solution)/shard_map/reduce_scatter | solution.py:168
Sparse Core Ops, SparseCore 0:
  10.1 60.6 all-gather.5
  73.6 56.6 all-gather.7
  175.6 6.8 reduce-scatter.2
  185.1 142.5 all-gather.9
  330.2 139.5 all-gather.11
  472.4 180.2 all-gather.13
  666.7 6.3 reduce-scatter.4
where the time goes:
time: 685 us; the launch traced here: 684 us
  waiting for transfers between devices  589 us (86%)
  matrix products  45.1 us (7%)
  other arithmetic  16.4 us (2%)
  local copies, waits for them, and re-layouts  14.7 us (2%)
  between operations  13.7 us (2%)
    all_gather x1, waiting for transfers between devices, body(): lax.all_gather(down_weight, 'sp', axis=1, tiled=True)  183 us
    all_gather x1, waiting for transfers between devices, body(): lax.all_gather(gate_weight, 'sp', axis=0, tiled=True)  141 us
    all_gather x1, waiting for transfers between devices, body(): lax.all_gather(up_weight, 'sp', axis=0, tiled=True)  134 us
    all_gather x1, waiting for transfers between devices, body(): lax.all_gather(values, 'sp', axis=0, tiled=True)  59.5 us
    all_gather x1, waiting for transfers between devices, body(): lax.all_gather(key_turned, 'sp', axis=0, tiled=True)  57.5 us
    dot_general x1, matrix products, body(): terms = jnp.dot(hidden, down_full, preferred_element_type=jnp.float32)  13.8 us
  transfers between devices with their start and end apart: 7, of which 7 were waited for; matrix products, arithmetic and copies ran while one was open for 2% of the time, Pallas kernels for 0%

commit v1 on v0

--- a/solution.py
+++ b/solution.py
@@ -75,7 +75,9 @@
     gate_full, up_full, down_full = (
         lax.all_gather(gate_weight, "sp", axis=0, tiled=True),
         lax.all_gather(up_weight, "sp", axis=0, tiled=True),
-        lax.all_gather(down_weight, "sp", axis=1, tiled=True),
+        jnp.concatenate(
+            lax.all_to_all(jnp.stack([down_weight] * lax.axis_size("sp")), "sp", 0, 0), axis=1
+        ),
     )
     places = lax.axis_index("sp") * own + jnp.arange(own, dtype=jnp.int32)
     grid_rows = places // GRID_W

time: 685 us -> 714 us (1.042)
  waiting for transfers between devices: 589 us -> 605 us
    all_gather x1, waiting for transfers between devices: 141 us -> 339 us  [body(): lax.all_gather(gate_weight, 'sp', axis=0, tiled=True)]
    all_gather x1 -> x0, waiting for transfers between devices: 183 us -> none  [body(): lax.all_gather(down_weight, 'sp', axis=1, tiled=True)]
  transfers between devices with their start and end apart: 7 -> 7, of which waited for: 7 -> 5; matrix products, arithmetic and copies ran while one was open for 2% -> 3% of each run, Pallas kernels for 0% -> 0%
where the time goes in v1:
time: 714 us; the launch traced here: 713 us
  waiting for transfers between devices  605 us (85%)
  matrix products  46.5 us (7%)
  local copies, waits for them, and re-layouts  21.5 us (3%)
  other arithmetic  16.3 us (2%)
  between operations  13.7 us (2%)
    all_gather x1, waiting for transfers between devices, body(): lax.all_gather(gate_weight, 'sp', axis=0, tiled=True)  339 us
    all_gather x1, waiting for transfers between devices, body(): lax.all_gather(up_weight, 'sp', axis=0, tiled=True)  141 us
    all_gather x1, waiting for transfers between devices, body(): lax.all_gather(values, 'sp', axis=0, tiled=True)  59.5 us
    all_gather x1, waiting for transfers between devices, body(): lax.all_gather(key_turned, 'sp', axis=0, tiled=True)  57.5 us
    dot_general x1, matrix products, body(): terms = jnp.dot(hidden, down_full, preferred_element_type=jnp.float32)  15.2 us
  transfers between devices with their start and end apart: 7, of which 5 were waited for; matrix products, arithmetic and copies ran while one was open for 3% of the time, Pallas kernels for 0%

profile of v1, /device:TPU:0, one launch (start us, length us, event | category | flops | bytes accessed | tf_op | source)
XLA Modules:
  0.0 712.9 jit_solution(11170191835093642015)
XLA Ops:
  6.6 1.1 copy.23
  7.8 0.8 fusion.22
  8.6 0.2 multiply_cosine_fusion.1
  8.8 0.7 copy.24
  9.6 0.0 all-gather.7.cloned.1.call-start
  9.7 0.7 all-gather.7.cloned.1.call-update
  10.4 0.0 reduce-scatter.3.cloned.1.call-start
  10.4 1.1 copy.25
  11.5 0.1 fusion.19
  11.6 0.8 fusion.20
  12.4 0.1 subtract_convert_fusion.1
  12.5 0.7 pad_maximum_fusion
  13.3 57.5 %all-gather.5.cloned.1.call-done = bf16[3072,256]{1,0:T(8,128)(2,1)} async-done(((bf16[192,256]{1,0:T(8,128)(2,1)}), bf16[3072,256]{1,0:T(8,128)(2,1)}) %all-gather.5.cloned.1.call-update) | async-done | bytes 1572880 | tf_op jit(solution)/shard_map/all_gather | solution.py:147
  70.8 59.5 %all-gather.7.cloned.1.call-done = bf16[3072,256]{1,0:T(8,128)(2,1)} async-done(((bf16[192,256]{1,0:T(8,128)(2,1)}), bf16[3072,256]{1,0:T(8,128)(2,1)}) %all-gather.7.cloned.1.call-update) | async-done | bytes 1572880 | tf_op jit(solution)/shard_map/all_gather | solution.py:148
  130.3 43.5 %while.15 = (s32[]{:T(128)}, f32[192,4,2]{0,2,1:T(2,128)S(1)}, f32[192,4,2]{0,2,1:T(2,128)S(1)}, f32[192,4,2,64]{0,3,2,1:T(8,128)S(1)}, bf16[2,1536,256]{2,1,0:T...) while((s32[]{:T(128)}, f32[192,4,2]{0,2,1:T(2,128)S(1)}, ...), condition=%wide.region_5.6_spmd.clone, body=%wide.region_2.5_spmd.clone.sunk | while | flops 623156736 | bytes 37257324 | solution.py:136
  130.3 2.6 constant_dynamic-slice_fusion.3
  132.9 1.4 copy.35
  134.3 6.0 bitcast_reduce_fusion.2
  140.4 5.4 fusion.51
  145.8 1.4 copy.36
  147.2 4.8 fusion.53
  152.1 2.6 constant_dynamic-slice_fusion.3
  154.7 1.4 copy.35
  156.1 6.0 bitcast_reduce_fusion.2
  162.1 5.4 fusion.51
  167.6 1.4 copy.36
  169.0 4.8 fusion.53
  173.8 0.1 divide_convert_fusion
  173.9 1.5 convolution_convert_fusion.1
  175.4 0.0 all-gather.9.cloned.1.call-start
  175.5 0.5 all-gather.9.cloned.1.call-update
  176.0 1.4 copy.28
  177.4 5.4 stack.2
  182.8 5.0 all-to-all-start
  187.8 0.0 all-gather.11.cloned.1.call-start
  187.8 0.5 all-gather.11.cloned.1.call-update
  188.4 0.0 reduce-scatter.5.cloned.1.call-start
  188.5 1.2 fusion.15
  189.7 0.2 fusion.17
  189.9 2.5 all_gather.20
  192.5 338.7 %all-gather.9.cloned.1.call-done = bf16[2048,2816]{1,0:T(8,128)(2,1)} async-done(((bf16[128,2816]{1,0:T(8,128)(2,1)}), bf16[2048,2816]{1,0:T(8,128)(2,1)}) %all-gather.9.cloned.1.call-update) | async-done | bytes 11534352 | tf_op jit(solution)/shard_map/all_gather | solution.py:76
  531.1 8.1 %fusion.27 = f32[192,2816]{1,0:T(8,128)} fusion(bf16[192,2048]{1,0:T(8,128)(2,1)S(1)} %all_gather.20, bf16[2048,2816]{1,0:T(8,128)(2,1)} %all-gather.9.cloned.1.call-done), kind=kOutput, calls=%fused_computation.67 | convolution fusion | flops 2214592512 | bytes 14483456 | tf_op jit(solution)/shard_map/dot_general | solution.py:166
  539.2 140.7 %all-gather.11.cloned.1.call-done = bf16[2048,2816]{1,0:T(8,128)(2,1)} async-done(((bf16[128,2816]{1,0:T(8,128)(2,1)}), bf16[2048,2816]{1,0:T(8,128)(2,1)}) %all-gather.11.cloned.1.call-update) | async-done | bytes 11534352 | tf_op jit(solution)/shard_map/all_gather | solution.py:77
  679.9 15.2 %convolution_convert_fusion = bf16[192,2048]{1,0:T(8,128)(2,1)} fusion(bf16[2816,2048]{0,1:T(8,128)(2,1)} %bitcast.13, bf16[192,2048]{1,0:T(8,128)(2,1)S(1)} %all_gather.20, bf16[2048,2816]{1,0:T(8,128)(2,1)} %all-gather.11.cloned.1.call-done, f32[192,2816]{1,0:T(8,128)} %fusion.27), kind=kOutput, calls=%fused_computation.19 | convolution fusion | flops 4432822272 | bytes 26804224 | tf_op jit(solution)/shard_map/dot_general | solution.py:169
  695.2 6.5 reduce-scatter.5.cloned.1.call-done
  701.7 1.1 fusion.18
  702.8 2.4 all_gather.23
  705.1 0.9 copy.50
  (29 shorter events, 0.3 us)
Async XLA Ops:
  6.5 167.4 %copy-start = (bf16[512,2048]{1,0:T(8,128)(2,1)S(1)}, bf16[512,2048]{1,0:T(8,128)(2,1)}, u32[]{:S(2)}) copy-start(bf16[512,2048]{1,0:T(8,128)(2,1)} %param.18) | copy-start | bytes 6291460
  6.5 64.3 %all-gather.5.cloned.1.call-start = ((), (), s32[]{:S(2)}) async-start(), calls=%async_computation.3 | async-start | bytes 1671168 | tf_op jit(solution)/shard_map/all_gather | solution.py:147
  9.6 120.7 %all-gather.7.cloned.1.call-start = ((), (), s32[]{:S(2)}) async-start(), calls=%async_computation.4 | async-start | bytes 1671168 | tf_op jit(solution)/shard_map/all_gather | solution.py:148
  10.4 178.1 %reduce-scatter.3.cloned.1.call-start = ((), (), s32[]{:S(2)}) async-start(), calls=%async_computation.5 | async-start | bytes 1179648 | tf_op jit(solution)/shard_map/reduce_scatter | solution.py:153
  175.4 355.7 %all-gather.9.cloned.1.call-start = ((), (), s32[]{:S(2)}) async-start(), calls=%async_computation.6 | async-start | bytes 12255232 | tf_op jit(solution)/shard_map/all_gather | solution.py:76
  182.8 5.7 copy-start.1
  182.8 7.0 copy-start.2
  182.8 356.4 %all-to-all-start = ((bf16[16,2816,128]{1,2,0:T(8,128)(2,1)}), bf16[16,2816,128]{1,2,0:T(8,128)(2,1)}, u32[]{:S(2)}, u32[]{:S(2)}) async-start(bf16[16,2816,128]{1,2,0:T(8,128)(2,1)} %stack.2), calls=%async_computation.1 | async-start | bytes 23068672 | tf_op jit(solution)/shard_map/all_to_all | solution.py:79
  187.8 492.1 %all-gather.11.cloned.1.call-start = ((), (), s32[]{:S(2)}) async-start(), calls=%async_computation.7 | async-start | bytes 12255232 | tf_op jit(solution)/shard_map/all_gather | solution.py:77
  188.4 513.3 %reduce-scatter.5.cloned.1.call-start = ((), (), s32[]{:S(2)}) async-start(), calls=%async_computation.8 | async-start | bytes 1179648 | tf_op jit(solution)/shard_map/reduce_scatter | solution.py:170
Sparse Core Ops, SparseCore 0:
  10.1 60.6 all-gather.4
  73.6 56.6 all-gather.6
  175.5 6.8 reduce-scatter.2
  185.1 346.0 all-gather.8
  533.7 146.1 all-gather.10
  695.3 6.3 reduce-scatter.4
